TPU v7x, 256 devices: a whole 4x4x8 slice. The times are simulated.
256 devices in a mesh: sp: 32 (over z, y), tp: 8 (over x, core).
Axes of the slice: x: 4, y: 4, z: 8, core: 2. Of those that a mesh axis runs over, the one named last changes fastest.
Arguments:
- residual_in: bfloat16 [12288, 2048], P(('sp', 'tp')), may hold values from -6 to 6
- queries: bfloat16 [12288, 2048], P('sp', 'tp'), may hold values from -180 to 180
- keys: bfloat16 [12288, 2048], P('sp', 'tp'), may hold values from -9 to 9
- values: bfloat16 [12288, 2048], P('sp', 'tp'), may hold values from -6 to 6
- mix_lambda: float32 [16], P('tp'), may hold values from 0.3 to 0.8
- head_gain: float32 [128], replicated, may hold values from 0.1 to 1.9
- out_weight: bfloat16 [2048, 2048], P('tp'), may hold values from -0.125 to 0.125
- norm_gain: float32 [2048], replicated, may hold values from 0.1 to 1.9
- gate_weight: bfloat16 [2048, 5632], P('sp', 'tp'), may hold values from -0.125 to 0.125
- up_weight: bfloat16 [2048, 5632], P('sp', 'tp'), may hold values from -0.125 to 0.125
- down_weight: bfloat16 [5632, 2048], P('tp', 'sp'), may hold values from -0.078125 to 0.078125
Outputs:
- layer_out: bfloat16 [12288, 2048], P(('sp', 'tp'))
All inputs are finite; a program needn't handle non-finite values.
Results may differ from a plain program's by a relative error of at most 0.014.
Values may be sent and summed in bfloat16 or wider, within the bound.
No kernel may reach another device: no remote copies, remote signals or barrier semaphores. Data moves between devices by JAX's collectives and lax.ppermute only.
A program may use at most 128 MiB of HBM per device.

v0:
```python
import math
import jax
import jax.numpy as jnp
from jax import lax
from jax.sharding import PartitionSpec as P

DH = 64
VD = 128


def cut_along(value, dim, devices):
    shape = value.shape
    parts = value.reshape(*shape[:dim], devices, shape[dim] // devices, *shape[dim + 1 :])
    return jnp.moveaxis(parts, dim, 0)


def sent_and_summed(value, axis, dim):
    parts = cut_along(value, dim, lax.axis_size(axis))
    arrived = lax.all_to_all(parts, axis, split_axis=0, concat_axis=0, tiled=True)
    return arrived.astype(jnp.float32).sum(axis=0)


def sent_to_all(value, axis):
    copies = jnp.broadcast_to(value, (lax.axis_size(axis), *value.shape))
    return lax.all_to_all(copies, axis, split_axis=0, concat_axis=0, tiled=True)


def joined_along(parts, dim):
    shape = list(parts.shape[1:])
    shape[dim] *= parts.shape[0]
    return jnp.moveaxis(parts, 0, dim).reshape(shape)


def collect(value, axis, dim):
    parts = sent_to_all(value, axis)
    return joined_along(parts, dim)


def rows_first(arrays, axis, dims):
    turned = [jnp.moveaxis(a, dim, 0) for a, dim in zip(arrays, dims)]
    widths = [t[0].size for t in turned]
    both = jnp.concatenate([t.reshape(-1, w) for t, w in zip(turned, widths)], axis=1)
    result = lax.all_gather(both, axis, axis=0, tiled=True)
    parts = jnp.split(result, [sum(widths[:k]) for k in range(1, len(widths))], axis=1)
    return tuple(
        (
            jnp.moveaxis(b.reshape(-1, *t.shape[1:]), 0, dim)
            for b, t, dim in zip(parts, turned, dims)
        )
    )


def body(
    residual_in,
    queries,
    keys,
    values,
    mix_lambda,
    head_gain,
    out_weight,
    norm_gain,
    gate_weight,
    up_weight,
    down_weight,
):
    tok_local = queries.shape[0]
    heads_local = mix_lambda.shape[0]
    query_four = queries.reshape(tok_local, heads_local, 2, DH)
    inverse_root = 1.0 / math.sqrt(DH)

    def one_block(state, block):
        top, total, weighted = state
        key_block, value_block = block
        scores = (
            jnp.einsum("qhcd,khcd->hcqk", query_four, key_block, preferred_element_type=jnp.float32)
            * inverse_root
        )
        new_top = jnp.maximum(top, jnp.max(scores, axis=-1))
        rescale = jnp.exp(top - new_top)
        expo = jnp.exp(scores - new_top[..., None])
        total = total * rescale + jnp.sum(expo, axis=-1)
        weighted = weighted * rescale[..., None] + jnp.einsum(
            "hcqk,khe->hcqe",
            expo.astype(jnp.bfloat16),
            value_block,
            preferred_element_type=jnp.float32,
        )
        return ((new_top, total, weighted), None)

    start_state = (
        jnp.full((heads_local, 2, tok_local), -1e30, jnp.float32),
        jnp.zeros((heads_local, 2, tok_local), jnp.float32),
        jnp.zeros((heads_local, 2, tok_local, VD), jnp.float32),
    )
    key_piece = lax.all_gather(keys, "sp", axis=0, tiled=True)
    value_piece = lax.all_gather(values, "sp", axis=0, tiled=True)
    count = key_piece.shape[0]
    shards = max(count // tok_local, 1)
    unit = count // shards
    group = max(
        (g for g in range(1, shards + 1) if shards % g == 0 and g * unit <= max(1536, unit))
    )
    width = group * unit
    blocks = count // width
    key_blocks = key_piece.reshape(blocks, width, heads_local, 2, DH)
    value_blocks = value_piece.reshape(blocks, width, heads_local, VD)
    state, unused = lax.scan(one_block, start_state, (key_blocks, value_blocks))
    top, total, weighted = state
    maps = weighted / total[..., None]
    mixed = maps[:, 0] - mix_lambda[:, None, None] * maps[:, 1]
    head_scale = lax.rsqrt(jnp.mean(mixed * mixed, axis=-1, keepdims=True) + 1e-06)
    head_out = (mixed * head_scale * head_gain).astype(jnp.bfloat16)
    attended = jnp.transpose(head_out, (1, 0, 2)).reshape(tok_local, heads_local * VD)
    picked = attended
    projected = sent_and_summed(
        jnp.dot(picked, out_weight, preferred_element_type=jnp.float32).astype(jnp.bfloat16),
        "tp",
        0,
    )
    after_mix = residual_in.astype(jnp.float32) + projected
    row_scale = lax.rsqrt(jnp.mean(after_mix * after_mix, axis=-1, keepdims=True) + 1e-06)
    normed = (after_mix * row_scale * norm_gain).astype(jnp.bfloat16)
    all_rows = collect(normed, "tp", 0)
    gate_all, up_all, down_all = rows_first((gate_weight, up_weight, down_weight), "sp", (0, 0, 1))
    gate = jnp.dot(all_rows, gate_all, preferred_element_type=jnp.float32)
    up = jnp.dot(all_rows, up_all, preferred_element_type=jnp.float32)
    hidden = (jax.nn.silu(gate) * up).astype(jnp.bfloat16)
    picked = hidden
    mixer = sent_and_summed(
        jnp.dot(picked, down_all, preferred_element_type=jnp.float32).astype(jnp.bfloat16), "tp", 0
    )
    return (after_mix + 0.5 * mixer).astype(jnp.bfloat16)


def solution(mesh):
    return jax.shard_map(
        body,
        mesh=mesh,
        in_specs=(
            P(("sp", "tp"), None),
            P("sp", "tp"),
            P("sp", "tp"),
            P("sp", "tp"),
            P("tp"),
            P(),
            P("tp", None),
            P(),
            P("sp", "tp"),
            P("sp", "tp"),
            P("tp", "sp"),
        ),
        out_specs=P(("sp", "tp"), None),
        check_vma=False,
    )
```

profile of v0, /device:TPU:1, one launch (start us, length us, event | category | flops | bytes accessed | tf_op | source)
XLA Modules:
  0.0 425.4 jit_solution(3736161622382868444)
XLA Ops:
  6.5 0.7 all-gather.4.cloned.1.call-update
  7.3 0.0 all-gather.6.cloned.1.call-start
  7.3 0.7 all-gather.6.cloned.1.call-update
  8.0 0.0 all-gather.8.cloned.1.call-start
  8.1 1.9 concatenate.3
  9.9 0.0 all-gather.8.cloned.1.call-update
  10.0 1.1 copy.17
  11.1 89.9 %all-gather.4.cloned.1.call-done = bf16[12288,256]{1,0:T(8,128)(2,1)} async-done(((bf16[384,256]{1,0:T(8,128)(2,1)}), bf16[12288,256]{1,0:T(8,128)(2,1)}) %all-gather.4.cloned.1.call-update) | async-done | bytes 6291472 | tf_op jit(solution)/shard_map/all_gather | solution.py:95
  101.0 21.8 %reshape.51 = bf16[8,1536,2,2,64]{4,3,2,1,0:T(2,128)(2,1)} reshape(bf16[12288,256]{1,0:T(8,128)(2,1)} %all-gather.4.cloned.1.call-done) | data formatting | bytes 12582912 | tf_op jit(solution)/shard_map/reshape | solution.py:105
  122.8 29.8 %copy.19 = bf16[8,1536,2,2,64]{1,4,3,2,0:T(8,128)(2,1)} copy(bf16[8,1536,2,2,64]{4,3,2,1,0:T(2,128)(2,1)} %reshape.51) | data formatting | bytes 12582912
  152.6 36.1 %all-gather.6.cloned.1.call-done = bf16[12288,256]{1,0:T(8,128)(2,1)} async-done(((bf16[384,256]{1,0:T(8,128)(2,1)}), bf16[12288,256]{1,0:T(8,128)(2,1)}) %all-gather.6.cloned.1.call-update) | async-done | bytes 6291472 | tf_op jit(solution)/shard_map/all_gather | solution.py:96
  188.7 9.7 %reshape.52 = bf16[8,1536,2,128]{3,2,1,0:T(2,128)(2,1)} reshape(bf16[12288,256]{1,0:T(8,128)(2,1)} %all-gather.6.cloned.1.call-done) | data formatting | bytes 12582912 | tf_op jit(solution)/shard_map/reshape | solution.py:106
  198.5 128.2 %while.15 = (s32[]{:T(128)}, f32[2,2,384]{2,1,0:T(2,128)S(1)}, f32[2,2,384]{2,1,0:T(2,128)S(1)}, f32[2,2,384,128]{3,2,1,0:T(8,128)S(1)}, bf16[8,1536,2,2,64]{1,4...) while((s32[]{:T(128)}, f32[2,2,384]{2,1,0:T(2,128)S(1)}, ...), condition=%wide.region_3.4_spmd.clone, body=%wide.region_0.3_spmd.clone.sunk | while | flops 925441536 | bytes 71074440 | solution.py:107
  198.5 6.2 %bitcast_reduce_fusion.2 = (f32[2,2,384]{2,1,0:T(2,128)S(1)}, f32[2,2,1536,384]{3,2,1,0:T(8,128)}) fusion(bf16[384,2,2,64]{0,3,2,1:T(8,128)(2,1)S(1)} %get-tuple-element.168, bf16[8,1536,2,2,64]{1,4,3,2,0:T(8,128)(2,1)} %get-tuple-element.167, s32[]{:T(128)} %get-tuple-element.154), kind=kOutput, calls=%fused_computation.1.clone.1 | convolution fusion | flops 306706944 | bytes 10426880 | tf_op jit(solution)/shard_map/while/body/eval_jaxpr/qhcd,khcd->hcqk/dot_general | solution.py:75
  204.7 5.4 %fusion.55 = f32[2,2,384]{2,1,0:T(2,128)S(1)} fusion(f32[2,2,1536,384]{3,2,1,0:T(8,128)} %get-tuple-element.142, f32[2,2,384]{2,1,0:T(2,128)S(1)} %fusion.54), kind=kLoop, calls=%fused_computation.4.clone.1 | loop fusion | flops 7076352 | bytes 9449472 | tf_op jit(solution)/shard_map/while/body/eval_jaxpr/reduce_sum | solution.py:81
  210.2 1.6 constant_dynamic-slice_fusion.2
  211.8 2.6 fusion.57
  214.4 6.2 %bitcast_reduce_fusion.2 = (f32[2,2,384]{2,1,0:T(2,128)S(1)}, f32[2,2,1536,384]{3,2,1,0:T(8,128)}) fusion(bf16[384,2,2,64]{0,3,2,1:T(8,128)(2,1)S(1)} %get-tuple-element.168, bf16[8,1536,2,2,64]{1,4,3,2,0:T(8,128)(2,1)} %get-tuple-element.167, s32[]{:T(128)} %get-tuple-element.154), kind=kOutput, calls=%fused_computation.1.clone.1 | convolution fusion | flops 306706944 | bytes 10426880 | tf_op jit(solution)/shard_map/while/body/eval_jaxpr/qhcd,khcd->hcqk/dot_general | solution.py:75
  220.7 5.4 %fusion.55 = f32[2,2,384]{2,1,0:T(2,128)S(1)} fusion(f32[2,2,1536,384]{3,2,1,0:T(8,128)} %get-tuple-element.142, f32[2,2,384]{2,1,0:T(2,128)S(1)} %fusion.54), kind=kLoop, calls=%fused_computation.4.clone.1 | loop fusion | flops 7076352 | bytes 9449472 | tf_op jit(solution)/shard_map/while/body/eval_jaxpr/reduce_sum | solution.py:81
  226.1 1.6 constant_dynamic-slice_fusion.2
  227.7 2.6 fusion.57
  230.4 6.2 %bitcast_reduce_fusion.2 = (f32[2,2,384]{2,1,0:T(2,128)S(1)}, f32[2,2,1536,384]{3,2,1,0:T(8,128)}) fusion(bf16[384,2,2,64]{0,3,2,1:T(8,128)(2,1)S(1)} %get-tuple-element.168, bf16[8,1536,2,2,64]{1,4,3,2,0:T(8,128)(2,1)} %get-tuple-element.167, s32[]{:T(128)} %get-tuple-element.154), kind=kOutput, calls=%fused_computation.1.clone.1 | convolution fusion | flops 306706944 | bytes 10426880 | tf_op jit(solution)/shard_map/while/body/eval_jaxpr/qhcd,khcd->hcqk/dot_general | solution.py:75
  236.6 5.6 %fusion.55 = f32[2,2,384]{2,1,0:T(2,128)S(1)} fusion(f32[2,2,1536,384]{3,2,1,0:T(8,128)} %get-tuple-element.142, f32[2,2,384]{2,1,0:T(2,128)S(1)} %fusion.54), kind=kLoop, calls=%fused_computation.4.clone.1 | loop fusion | flops 7076352 | bytes 9449472 | tf_op jit(solution)/shard_map/while/body/eval_jaxpr/reduce_sum | solution.py:81
  242.2 1.9 constant_dynamic-slice_fusion.2
  244.1 2.6 fusion.57
  246.8 6.2 %bitcast_reduce_fusion.2 = (f32[2,2,384]{2,1,0:T(2,128)S(1)}, f32[2,2,1536,384]{3,2,1,0:T(8,128)}) fusion(bf16[384,2,2,64]{0,3,2,1:T(8,128)(2,1)S(1)} %get-tuple-element.168, bf16[8,1536,2,2,64]{1,4,3,2,0:T(8,128)(2,1)} %get-tuple-element.167, s32[]{:T(128)} %get-tuple-element.154), kind=kOutput, calls=%fused_computation.1.clone.1 | convolution fusion | flops 306706944 | bytes 10426880 | tf_op jit(solution)/shard_map/while/body/eval_jaxpr/qhcd,khcd->hcqk/dot_general | solution.py:75
  253.0 5.6 %fusion.55 = f32[2,2,384]{2,1,0:T(2,128)S(1)} fusion(f32[2,2,1536,384]{3,2,1,0:T(8,128)} %get-tuple-element.142, f32[2,2,384]{2,1,0:T(2,128)S(1)} %fusion.54), kind=kLoop, calls=%fused_computation.4.clone.1 | loop fusion | flops 7076352 | bytes 9449472 | tf_op jit(solution)/shard_map/while/body/eval_jaxpr/reduce_sum | solution.py:81
  258.7 1.6 constant_dynamic-slice_fusion.2
  260.3 2.6 fusion.57
  263.0 6.2 %bitcast_reduce_fusion.2 = (f32[2,2,384]{2,1,0:T(2,128)S(1)}, f32[2,2,1536,384]{3,2,1,0:T(8,128)}) fusion(bf16[384,2,2,64]{0,3,2,1:T(8,128)(2,1)S(1)} %get-tuple-element.168, bf16[8,1536,2,2,64]{1,4,3,2,0:T(8,128)(2,1)} %get-tuple-element.167, s32[]{:T(128)} %get-tuple-element.154), kind=kOutput, calls=%fused_computation.1.clone.1 | convolution fusion | flops 306706944 | bytes 10426880 | tf_op jit(solution)/shard_map/while/body/eval_jaxpr/qhcd,khcd->hcqk/dot_general | solution.py:75
  269.2 5.4 %fusion.55 = f32[2,2,384]{2,1,0:T(2,128)S(1)} fusion(f32[2,2,1536,384]{3,2,1,0:T(8,128)} %get-tuple-element.142, f32[2,2,384]{2,1,0:T(2,128)S(1)} %fusion.54), kind=kLoop, calls=%fused_computation.4.clone.1 | loop fusion | flops 7076352 | bytes 9449472 | tf_op jit(solution)/shard_map/while/body/eval_jaxpr/reduce_sum | solution.py:81
  274.7 1.6 constant_dynamic-slice_fusion.2
  276.3 2.6 fusion.57
  279.0 6.2 %bitcast_reduce_fusion.2 = (f32[2,2,384]{2,1,0:T(2,128)S(1)}, f32[2,2,1536,384]{3,2,1,0:T(8,128)}) fusion(bf16[384,2,2,64]{0,3,2,1:T(8,128)(2,1)S(1)} %get-tuple-element.168, bf16[8,1536,2,2,64]{1,4,3,2,0:T(8,128)(2,1)} %get-tuple-element.167, s32[]{:T(128)} %get-tuple-element.154), kind=kOutput, calls=%fused_computation.1.clone.1 | convolution fusion | flops 306706944 | bytes 10426880 | tf_op jit(solution)/shard_map/while/body/eval_jaxpr/qhcd,khcd->hcqk/dot_general | solution.py:75
  285.2 5.4 %fusion.55 = f32[2,2,384]{2,1,0:T(2,128)S(1)} fusion(f32[2,2,1536,384]{3,2,1,0:T(8,128)} %get-tuple-element.142, f32[2,2,384]{2,1,0:T(2,128)S(1)} %fusion.54), kind=kLoop, calls=%fused_computation.4.clone.1 | loop fusion | flops 7076352 | bytes 9449472 | tf_op jit(solution)/shard_map/while/body/eval_jaxpr/reduce_sum | solution.py:81
  290.6 1.6 constant_dynamic-slice_fusion.2
  292.2 2.6 fusion.57
  294.9 6.2 %bitcast_reduce_fusion.2 = (f32[2,2,384]{2,1,0:T(2,128)S(1)}, f32[2,2,1536,384]{3,2,1,0:T(8,128)}) fusion(bf16[384,2,2,64]{0,3,2,1:T(8,128)(2,1)S(1)} %get-tuple-element.168, bf16[8,1536,2,2,64]{1,4,3,2,0:T(8,128)(2,1)} %get-tuple-element.167, s32[]{:T(128)} %get-tuple-element.154), kind=kOutput, calls=%fused_computation.1.clone.1 | convolution fusion | flops 306706944 | bytes 10426880 | tf_op jit(solution)/shard_map/while/body/eval_jaxpr/qhcd,khcd->hcqk/dot_general | solution.py:75
  301.1 5.4 %fusion.55 = f32[2,2,384]{2,1,0:T(2,128)S(1)} fusion(f32[2,2,1536,384]{3,2,1,0:T(8,128)} %get-tuple-element.142, f32[2,2,384]{2,1,0:T(2,128)S(1)} %fusion.54), kind=kLoop, calls=%fused_computation.4.clone.1 | loop fusion | flops 7076352 | bytes 9449472 | tf_op jit(solution)/shard_map/while/body/eval_jaxpr/reduce_sum | solution.py:81
  306.5 1.6 constant_dynamic-slice_fusion.2
  308.1 2.6 fusion.57
  310.8 6.2 %bitcast_reduce_fusion.2 = (f32[2,2,384]{2,1,0:T(2,128)S(1)}, f32[2,2,1536,384]{3,2,1,0:T(8,128)}) fusion(bf16[384,2,2,64]{0,3,2,1:T(8,128)(2,1)S(1)} %get-tuple-element.168, bf16[8,1536,2,2,64]{1,4,3,2,0:T(8,128)(2,1)} %get-tuple-element.167, s32[]{:T(128)} %get-tuple-element.154), kind=kOutput, calls=%fused_computation.1.clone.1 | convolution fusion | flops 306706944 | bytes 10426880 | tf_op jit(solution)/shard_map/while/body/eval_jaxpr/qhcd,khcd->hcqk/dot_general | solution.py:75
  317.0 5.4 %fusion.55 = f32[2,2,384]{2,1,0:T(2,128)S(1)} fusion(f32[2,2,1536,384]{3,2,1,0:T(8,128)} %get-tuple-element.142, f32[2,2,384]{2,1,0:T(2,128)S(1)} %fusion.54), kind=kLoop, calls=%fused_computation.4.clone.1 | loop fusion | flops 7076352 | bytes 9449472 | tf_op jit(solution)/shard_map/while/body/eval_jaxpr/reduce_sum | solution.py:81
  322.4 1.6 constant_dynamic-slice_fusion.2
  324.0 2.6 fusion.57
  326.7 0.0 copy-start.4
  326.7 0.0 copy-start.5
  326.7 0.3 copy.22
  327.0 0.1 broadcast_divide_fusion
  327.1 0.3 copy-done.4
  327.4 0.1 multiply_reduce_fusion.1
  327.5 0.1 multiply_convert_fusion.1
  327.7 0.6 convolution_convert_fusion
  328.3 26.4 %all_to_all.15 = bf16[8,48,2048]{2,1,0:T(8,128)(2,1)S(1)} all-to-all(bf16[8,48,2048]{2,1,0:T(8,128)(2,1)S(1)} %bitcast.67), channel_id=1, replica_groups=mesh['sp'=32,'tp'=8] {'tp'}, dimensions={0} | all-to-all | bytes 3145728 | tf_op jit(solution)/shard_map/all_to_all | solution.py:19
  354.7 0.2 convert_reduce_fusion.1
  355.0 0.2 multiply_reduce_fusion
  355.1 0.1 multiply_convert_fusion
  355.2 0.2 broadcast_in_dim.13
  355.4 24.0 %all_to_all.16 = bf16[8,48,2048]{2,1,0:T(8,128)(2,1)S(1)} all-to-all(bf16[8,48,2048]{2,1,0:T(8,128)(2,1)S(1)} %broadcast_in_dim.13), channel_id=1, replica_groups=mesh['sp'=32,'tp'=8] {'tp'}, dimensions={0} | all-to-all | bytes 3145728 | tf_op jit(solution)/shard_map/all_to_all | solution.py:25
  379.5 4.6 %fusion.21 = f32[384,704]{0,1:T(8,128)} fusion(bf16[384,2048]{1,0:T(8,128)(2,1)S(1)} %bitcast.68, bf16[2048,2112]{1,0:T(8,128)(2,1)} %all-gather.8.cloned.1.call-done), kind=kOutput, calls=%fused_computation.26 | convolution fusion | flops 1107296256 | bytes 5799936 | tf_op jit(solution)/shard_map/dot_general | solution.py:125
  384.0 8.8 %fusion.23 = bf16[384,2048]{1,0:T(8,128)(2,1)} fusion(bf16[2048,2112]{1,0:T(8,128)(2,1)} %all-gather.8.cloned.1.call-done, bf16[384,2048]{1,0:T(8,128)(2,1)S(1)} %bitcast.69, f32[384,704]{0,1:T(8,128)} %fusion.21), kind=kOutput, calls=%fused_computation.30 | convolution fusion | flops 2217000960 | bytes 10518528 | tf_op jit(solution)/shard_map/dot_general | solution.py:130
  392.8 25.1 %all_to_all.17 = bf16[8,48,2048]{2,1,0:T(8,128)(2,1)S(1)} all-to-all(bf16[8,48,2048]{2,1,0:T(8,128)(2,1)} %bitcast.70), channel_id=1, replica_groups=mesh['sp'=32,'tp'=8] {'tp'}, dimensions={0} | all-to-all | bytes 3145728 | tf_op jit(solution)/shard_map/all_to_all | solution.py:19
  417.9 0.2 convert_reduce_fusion
  418.1 0.8 add_convert_fusion
  (55 shorter events, 0.4 us)
Async XLA Ops:
  6.5 321.1 %copy-start = (bf16[256,2048]{1,0:T(8,128)(2,1)S(1)}, bf16[256,2048]{1,0:T(8,128)(2,1)}, u32[]{:S(2)}) copy-start(bf16[256,2048]{1,0:T(8,128)(2,1)} %param.19) | copy-start | bytes 3145732
  6.5 94.5 %all-gather.4.cloned.1.call-start = ((), (), s32[]{:S(2)}) async-start(), calls=%async_computation.3 | async-start | bytes 6488064 | tf_op jit(solution)/shard_map/all_gather | solution.py:95
  7.3 181.5 %all-gather.6.cloned.1.call-start = ((), (), s32[]{:S(2)}) async-start(), calls=%async_computation.4 | async-start | bytes 6488064 | tf_op jit(solution)/shard_map/all_gather | solution.py:96
  8.0 371.5 %all-gather.8.cloned.1.call-start = ((), (), s32[]{:S(2)}) async-start(), calls=%async_computation.5 | async-start | bytes 9191424 | tf_op jit(solution)/shard_map/all_gather | solution.py:43
  204.7 7.1 %copy-start.1 = (f32[2,2,1536,384]{3,2,1,0:T(8,128)S(1)}, f32[2,2,1536,384]{3,2,1,0:T(8,128)}, u32[]{:S(2)}) copy-start(f32[2,2,1536,384]{3,2,1,0:T(8,128)} %get-tuple-element.142) | copy-start | bytes 28311556 | tf_op jit(solution)/shard_map/while
  220.7 7.1 %copy-start.1 = (f32[2,2,1536,384]{3,2,1,0:T(8,128)S(1)}, f32[2,2,1536,384]{3,2,1,0:T(8,128)}, u32[]{:S(2)}) copy-start(f32[2,2,1536,384]{3,2,1,0:T(8,128)} %get-tuple-element.142) | copy-start | bytes 28311556 | tf_op jit(solution)/shard_map/while
  236.6 7.5 %copy-start.1 = (f32[2,2,1536,384]{3,2,1,0:T(8,128)S(1)}, f32[2,2,1536,384]{3,2,1,0:T(8,128)}, u32[]{:S(2)}) copy-start(f32[2,2,1536,384]{3,2,1,0:T(8,128)} %get-tuple-element.142) | copy-start | bytes 28311556 | tf_op jit(solution)/shard_map/while
  253.0 7.3 %copy-start.1 = (f32[2,2,1536,384]{3,2,1,0:T(8,128)S(1)}, f32[2,2,1536,384]{3,2,1,0:T(8,128)}, u32[]{:S(2)}) copy-start(f32[2,2,1536,384]{3,2,1,0:T(8,128)} %get-tuple-element.142) | copy-start | bytes 28311556 | tf_op jit(solution)/shard_map/while
  269.2 7.1 %copy-start.1 = (f32[2,2,1536,384]{3,2,1,0:T(8,128)S(1)}, f32[2,2,1536,384]{3,2,1,0:T(8,128)}, u32[]{:S(2)}) copy-start(f32[2,2,1536,384]{3,2,1,0:T(8,128)} %get-tuple-element.142) | copy-start | bytes 28311556 | tf_op jit(solution)/shard_map/while
  285.2 7.0 %copy-start.1 = (f32[2,2,1536,384]{3,2,1,0:T(8,128)S(1)}, f32[2,2,1536,384]{3,2,1,0:T(8,128)}, u32[]{:S(2)}) copy-start(f32[2,2,1536,384]{3,2,1,0:T(8,128)} %get-tuple-element.142) | copy-start | bytes 28311556 | tf_op jit(solution)/shard_map/while
  301.1 7.0 %copy-start.1 = (f32[2,2,1536,384]{3,2,1,0:T(8,128)S(1)}, f32[2,2,1536,384]{3,2,1,0:T(8,128)}, u32[]{:S(2)}) copy-start(f32[2,2,1536,384]{3,2,1,0:T(8,128)} %get-tuple-element.142) | copy-start | bytes 28311556 | tf_op jit(solution)/shard_map/while
  317.0 7.0 %copy-start.1 = (f32[2,2,1536,384]{3,2,1,0:T(8,128)S(1)}, f32[2,2,1536,384]{3,2,1,0:T(8,128)}, u32[]{:S(2)}) copy-start(f32[2,2,1536,384]{3,2,1,0:T(8,128)} %get-tuple-element.142) | copy-start | bytes 28311556 | tf_op jit(solution)/shard_map/while
  326.7 0.7 copy-start.4
  326.7 0.8 copy-start.5
  328.3 26.7 %copy-start.2 = (bf16[48,2048]{1,0:T(8,128)(2,1)S(1)}, bf16[48,2048]{1,0:T(8,128)(2,1)}, u32[]{:S(2)}) copy-start(bf16[48,2048]{1,0:T(8,128)(2,1)} %param.13) | copy-start | bytes 589828
  328.3 26.8 %copy-start.3 = (f32[2048]{0:T(1024)S(1)}, f32[2048]{0:T(1024)}, u32[]{:S(2)}) copy-start(f32[2048]{0:T(1024)} %param.20) | copy-start | bytes 24580
Sparse Core Ops, SparseCore 0:
  9.9 91.0 all-gather.3
  103.6 85.0 all-gather.5
  191.3 97.5 all-gather.7
where the time goes:
time: 428 us; the launch traced here: 425 us
  waiting for transfers between devices  127 us (30%)
  matrix products  84.7 us (20%)
  local copies, waits for them, and re-layouts  78.1 us (18%)
  blocking collectives  75.5 us (18%)
  other arithmetic  45.7 us (11%)
  between operations  13.3 us (3%)
    all_gather x1, waiting for transfers between devices, body(): key_piece = lax.all_gather(keys, 'sp', axis=0, tiled=True)  89.9 us
    all_to_all x2, blocking collectives, sent_and_summed(): lax.all_to_all(parts, axis, split_axis=0, concat_axis=0, tiled=True)  51.5 us
    dot_general x8, matrix products, one_block(): jnp.einsum('qhcd,khcd->hcqk', query_four, key_block, preferred_element_ty...  49.6 us
    reduce_sum x8, other arithmetic, one_block(): total = total * rescale + jnp.sum(expo, axis=-1)  43.7 us
    all_gather x1, waiting for transfers between devices, body(): value_piece = lax.all_gather(values, 'sp', axis=0, tiled=True)  36.1 us
    unnamed x12, local copies, waits for them, and re-layouts  31.2 us
    all_to_all x1, blocking collectives, sent_to_all(): return lax.all_to_all(copies, axis, split_axis=0, concat_axis=0, tiled=True)  24 us
    reshape x1, local copies, waits for them, and re-layouts, body(): key_blocks = key_piece.reshape(blocks, width, heads_local, 2, DH)  21.8 us
  transfers between devices with their start and end apart: 3, of which 2 were waited for; matrix products, arithmetic and copies ran while one was open for 46% of the time, Pallas kernels for 0%

commit v1 on v0

--- a/solution.py
+++ b/solution.py
@@ -92,7 +92,13 @@
         jnp.zeros((heads_local, 2, tok_local), jnp.float32),
         jnp.zeros((heads_local, 2, tok_local, VD), jnp.float32),
     )
-    key_piece = lax.all_gather(keys, "sp", axis=0, tiled=True)
+    key_piece = lax.all_to_all(
+        jnp.concatenate([keys for _ in range(lax.axis_size("sp"))], axis=0),
+        axis_name="sp",
+        split_axis=0,
+        concat_axis=0,
+        tiled=True,
+    )
     value_piece = lax.all_gather(values, "sp", axis=0, tiled=True)
     count = key_piece.shape[0]
     shards = max(count // tok_local, 1)

time: 428 us -> 489 us (1.14)
  waiting for transfers between devices: 127 us -> 176 us
  starting transfers between devices: 0.08 us -> 12.3 us
    all_to_all x0 -> x1, waiting for transfers between devices: none -> 175 us  [body(): lax.all_to_all(jnp.concatenate([keys for _ in range(lax.axis_size('sp'))]...]
    all_gather x1 -> x0, waiting for transfers between devices: 89.9 us -> none  [body(): key_piece = lax.all_gather(keys, 'sp', axis=0, tiled=True)]
    all_gather x1, waiting for transfers between devices: 36.1 us -> 0.01 us  [body(): value_piece = lax.all_gather(values, 'sp', axis=0, tiled=True)]
    all_to_all x0 -> x2, local copies, waits for them, and re-layouts: none -> 17.8 us  [body(): lax.all_to_all(jnp.concatenate([keys for _ in range(lax.axis_size('sp'))]...]
    all_to_all x0 -> x1, starting transfers between devices: none -> 12.3 us  [body(): lax.all_to_all(jnp.concatenate([keys for _ in range(lax.axis_size('sp'))]...]
    reshape x1, local copies, waits for them, and re-layouts: 21.8 us -> 10.7 us  [body(): key_blocks = key_piece.reshape(blocks, width, heads_local, 2, DH)]
    unnamed x12 -> x55, local copies, waits for them, and re-layouts: 31.2 us -> 26.1 us
  transfers between devices with their start and end apart: 3 -> 3, of which waited for: 2 -> 1; matrix products, arithmetic and copies ran while one was open for 46% -> 39% of each run, Pallas kernels for 0% -> 0%
where the time goes in v1:
time: 489 us; the launch traced here: 487 us
  waiting for transfers between devices  176 us (36%)
  matrix products  84.2 us (17%)
  local copies, waits for them, and re-layouts  78.5 us (16%)
  blocking collectives  76.9 us (16%)
  other arithmetic  45.4 us (9%)
  between operations  13.8 us (3%)
  starting transfers between devices  12.3 us (3%)
    all_to_all x1, waiting for transfers between devices, body(): lax.all_to_all(jnp.concatenate([keys for _ in range(lax.axis_size('sp'))]...  175 us
    all_to_all x2, blocking collectives, sent_and_summed(): lax.all_to_all(parts, axis, split_axis=0, concat_axis=0, tiled=True)  52.2 us
    dot_general x8, matrix products, one_block(): jnp.einsum('qhcd,khcd->hcqk', query_four, key_block, preferred_element_ty...  49.5 us
    reduce_sum x8, other arithmetic, one_block(): total = total * rescale + jnp.sum(expo, axis=-1)  43.4 us
    unnamed x55, local copies, waits for them, and re-layouts  26.1 us
    all_to_all x1, blocking collectives, sent_to_all(): return lax.all_to_all(copies, axis, split_axis=0, concat_axis=0, tiled=True)  24.7 us
    dot_general x8, matrix products, one_block(): jnp.einsum('hcqk,khe->hcqe', expo.astype(jnp.bfloat16), value_block, pref...  21.2 us
    all_to_all x2, local copies, waits for them, and re-layouts, body(): lax.all_to_all(jnp.concatenate([keys for _ in range(lax.axis_size('sp'))]...  17.8 us
  transfers between devices with their start and end apart: 3, of which 1 were waited for; matrix products, arithmetic and copies ran while one was open for 39% of the time, Pallas kernels for 0%

profile of v1, /device:TPU:1, one launch (start us, length us, event | category | flops | bytes accessed | tf_op | source)
XLA Modules:
  0.0 487.4 jit_solution(12614421456332718405)
XLA Ops:
  7.3 0.9 constant_dynamic-update-slice_fusion.31
  8.2 0.9 constant_dynamic-update-slice_fusion.30
  9.2 0.9 constant_dynamic-update-slice_fusion.29
  10.1 0.9 constant_dynamic-update-slice_fusion.28
  11.0 0.9 constant_dynamic-update-slice_fusion.27
  12.0 0.9 constant_dynamic-update-slice_fusion.26
  12.9 0.9 constant_dynamic-update-slice_fusion.25
  13.9 0.9 constant_dynamic-update-slice_fusion.24
  14.8 0.9 constant_dynamic-update-slice_fusion.23
  15.8 0.9 constant_dynamic-update-slice_fusion.22
  16.7 0.9 constant_dynamic-update-slice_fusion.21
  17.7 0.9 constant_dynamic-update-slice_fusion.20
  18.6 0.9 constant_dynamic-update-slice_fusion.19
  19.6 0.9 constant_dynamic-update-slice_fusion.18
  20.5 0.9 constant_dynamic-update-slice_fusion.17
  21.4 0.9 constant_dynamic-update-slice_fusion.16
  22.8 2.6 copy-done.3
  25.4 8.6 %copy.32 = bf16[32,384,256]{1,2,0:T(8,128)(2,1)} copy(bf16[32,384,256]{2,1,0:T(8,128)(2,1)} %bitcast.70) | data formatting | bytes 12582912 | tf_op jit(solution)/shard_map/all_to_all | solution.py:95
  34.0 12.3 %all-to-all-start = ((bf16[32,384,256]{1,2,0:T(8,128)(2,1)}), bf16[32,384,256]{1,2,0:T(8,128)(2,1)}, u32[]{:S(2)}, u32[]{:S(2)}) async-start(bf16[32,384,256]{1,2,0:T(8,128)(2,1)} %copy.32), calls=%async_computation | async-start | bytes 12582912 | tf_op jit(solution)/shard_map/all_to_all | solution.py:95
  46.3 0.8 concatenate.7
  47.4 175.1 %all-to-all-done = bf16[32,384,256]{1,2,0:T(8,128)(2,1)} async-done(((bf16[32,384,256]{1,2,0:T(8,128)(2,1)}), bf16[32,384,256]{1,2,0:T(8,128)(2,1)}, u32[]{:S(2)}, u32[]{:S(2)}) %all-to-all-start) | async-done | bytes 6291488 | tf_op jit(solution)/shard_map/all_to_all | solution.py:95
  222.5 9.2 %copy.33 = bf16[32,384,256]{1,0,2:T(8,128)(2,1)} copy(bf16[32,384,256]{1,2,0:T(8,128)(2,1)} %all-to-all-done) | data formatting | bytes 12582912 | tf_op jit(solution)/shard_map/all_to_all | solution.py:95
  231.7 10.7 %reshape.46 = bf16[8,1536,2,2,64]{1,0,4,3,2:T(8,128)(2,1)} reshape(bf16[32,384,256]{1,0,2:T(8,128)(2,1)} %copy.33) | data formatting | bytes 12582912 | tf_op jit(solution)/shard_map/reshape | solution.py:111
  242.3 8.0 %copy.36 = bf16[8,1536,2,2,64]{1,4,3,2,0:T(8,128)(2,1)} copy(bf16[8,1536,2,2,64]{1,0,4,3,2:T(8,128)(2,1)} %reshape.46) | data formatting | bytes 12582912
  250.3 9.8 %reshape.54 = bf16[8,1536,2,128]{3,2,1,0:T(2,128)(2,1)} reshape(bf16[12288,256]{1,0:T(8,128)(2,1)} %all-gather.3.cloned.1.call-done) | data formatting | bytes 12582912 | tf_op jit(solution)/shard_map/reshape | solution.py:112
  260.1 127.6 %while.15 = (s32[]{:T(128)}, f32[2,2,384]{2,1,0:T(2,128)S(1)}, f32[2,2,384]{2,1,0:T(2,128)S(1)}, f32[2,2,384,128]{3,2,1,0:T(8,128)S(1)}, bf16[8,1536,2,2,64]{1,4...) while((s32[]{:T(128)}, f32[2,2,384]{2,1,0:T(2,128)S(1)}, ...), condition=%wide.region_3.4_spmd.clone, body=%wide.region_0.3_spmd.clone.sunk | while | flops 925441536 | bytes 71074440 | solution.py:113
  260.1 6.2 %bitcast_reduce_fusion.2 = (f32[2,2,384]{2,1,0:T(2,128)S(1)}, f32[2,2,1536,384]{3,2,1,0:T(8,128)}) fusion(bf16[384,2,2,64]{0,3,2,1:T(8,128)(2,1)S(1)} %get-tuple-element.182, bf16[8,1536,2,2,64]{1,4,3,2,0:T(8,128)(2,1)} %get-tuple-element.181, s32[]{:T(128)} %get-tuple-element.168), kind=kOutput, calls=%fused_computation.1.clone.1 | convolution fusion | flops 306706944 | bytes 10426880 | tf_op jit(solution)/shard_map/while/body/eval_jaxpr/qhcd,khcd->hcqk/dot_general | solution.py:75
  266.3 5.6 %fusion.55 = f32[2,2,384]{2,1,0:T(2,128)S(1)} fusion(f32[2,2,1536,384]{3,2,1,0:T(8,128)} %get-tuple-element.156, f32[2,2,384]{2,1,0:T(2,128)S(1)} %fusion.54), kind=kLoop, calls=%fused_computation.4.clone.1 | loop fusion | flops 7076352 | bytes 9449472 | tf_op jit(solution)/shard_map/while/body/eval_jaxpr/reduce_sum | solution.py:81
  271.9 1.7 constant_dynamic-slice_fusion.2
  273.7 2.6 fusion.57
  276.3 6.2 %bitcast_reduce_fusion.2 = (f32[2,2,384]{2,1,0:T(2,128)S(1)}, f32[2,2,1536,384]{3,2,1,0:T(8,128)}) fusion(bf16[384,2,2,64]{0,3,2,1:T(8,128)(2,1)S(1)} %get-tuple-element.182, bf16[8,1536,2,2,64]{1,4,3,2,0:T(8,128)(2,1)} %get-tuple-element.181, s32[]{:T(128)} %get-tuple-element.168), kind=kOutput, calls=%fused_computation.1.clone.1 | convolution fusion | flops 306706944 | bytes 10426880 | tf_op jit(solution)/shard_map/while/body/eval_jaxpr/qhcd,khcd->hcqk/dot_general | solution.py:75
  282.6 5.5 %fusion.55 = f32[2,2,384]{2,1,0:T(2,128)S(1)} fusion(f32[2,2,1536,384]{3,2,1,0:T(8,128)} %get-tuple-element.156, f32[2,2,384]{2,1,0:T(2,128)S(1)} %fusion.54), kind=kLoop, calls=%fused_computation.4.clone.1 | loop fusion | flops 7076352 | bytes 9449472 | tf_op jit(solution)/shard_map/while/body/eval_jaxpr/reduce_sum | solution.py:81
  288.1 1.6 constant_dynamic-slice_fusion.2
  289.7 2.6 fusion.57
  292.4 6.2 %bitcast_reduce_fusion.2 = (f32[2,2,384]{2,1,0:T(2,128)S(1)}, f32[2,2,1536,384]{3,2,1,0:T(8,128)}) fusion(bf16[384,2,2,64]{0,3,2,1:T(8,128)(2,1)S(1)} %get-tuple-element.182, bf16[8,1536,2,2,64]{1,4,3,2,0:T(8,128)(2,1)} %get-tuple-element.181, s32[]{:T(128)} %get-tuple-element.168), kind=kOutput, calls=%fused_computation.1.clone.1 | convolution fusion | flops 306706944 | bytes 10426880 | tf_op jit(solution)/shard_map/while/body/eval_jaxpr/qhcd,khcd->hcqk/dot_general | solution.py:75
  298.6 5.4 %fusion.55 = f32[2,2,384]{2,1,0:T(2,128)S(1)} fusion(f32[2,2,1536,384]{3,2,1,0:T(8,128)} %get-tuple-element.156, f32[2,2,384]{2,1,0:T(2,128)S(1)} %fusion.54), kind=kLoop, calls=%fused_computation.4.clone.1 | loop fusion | flops 7076352 | bytes 9449472 | tf_op jit(solution)/shard_map/while/body/eval_jaxpr/reduce_sum | solution.py:81
  304.0 1.6 constant_dynamic-slice_fusion.2
  305.6 2.6 fusion.57
  308.3 6.2 %bitcast_reduce_fusion.2 = (f32[2,2,384]{2,1,0:T(2,128)S(1)}, f32[2,2,1536,384]{3,2,1,0:T(8,128)}) fusion(bf16[384,2,2,64]{0,3,2,1:T(8,128)(2,1)S(1)} %get-tuple-element.182, bf16[8,1536,2,2,64]{1,4,3,2,0:T(8,128)(2,1)} %get-tuple-element.181, s32[]{:T(128)} %get-tuple-element.168), kind=kOutput, calls=%fused_computation.1.clone.1 | convolution fusion | flops 306706944 | bytes 10426880 | tf_op jit(solution)/shard_map/while/body/eval_jaxpr/qhcd,khcd->hcqk/dot_general | solution.py:75
  314.5 5.4 %fusion.55 = f32[2,2,384]{2,1,0:T(2,128)S(1)} fusion(f32[2,2,1536,384]{3,2,1,0:T(8,128)} %get-tuple-element.156, f32[2,2,384]{2,1,0:T(2,128)S(1)} %fusion.54), kind=kLoop, calls=%fused_computation.4.clone.1 | loop fusion | flops 7076352 | bytes 9449472 | tf_op jit(solution)/shard_map/while/body/eval_jaxpr/reduce_sum | solution.py:81
  319.9 1.6 constant_dynamic-slice_fusion.2
  321.5 2.6 fusion.57
  324.2 6.2 %bitcast_reduce_fusion.2 = (f32[2,2,384]{2,1,0:T(2,128)S(1)}, f32[2,2,1536,384]{3,2,1,0:T(8,128)}) fusion(bf16[384,2,2,64]{0,3,2,1:T(8,128)(2,1)S(1)} %get-tuple-element.182, bf16[8,1536,2,2,64]{1,4,3,2,0:T(8,128)(2,1)} %get-tuple-element.181, s32[]{:T(128)} %get-tuple-element.168), kind=kOutput, calls=%fused_computation.1.clone.1 | convolution fusion | flops 306706944 | bytes 10426880 | tf_op jit(solution)/shard_map/while/body/eval_jaxpr/qhcd,khcd->hcqk/dot_general | solution.py:75
  330.3 5.4 %fusion.55 = f32[2,2,384]{2,1,0:T(2,128)S(1)} fusion(f32[2,2,1536,384]{3,2,1,0:T(8,128)} %get-tuple-element.156, f32[2,2,384]{2,1,0:T(2,128)S(1)} %fusion.54), kind=kLoop, calls=%fused_computation.4.clone.1 | loop fusion | flops 7076352 | bytes 9449472 | tf_op jit(solution)/shard_map/while/body/eval_jaxpr/reduce_sum | solution.py:81
  335.8 1.6 constant_dynamic-slice_fusion.2
  337.4 2.6 fusion.57
  340.0 6.2 %bitcast_reduce_fusion.2 = (f32[2,2,384]{2,1,0:T(2,128)S(1)}, f32[2,2,1536,384]{3,2,1,0:T(8,128)}) fusion(bf16[384,2,2,64]{0,3,2,1:T(8,128)(2,1)S(1)} %get-tuple-element.182, bf16[8,1536,2,2,64]{1,4,3,2,0:T(8,128)(2,1)} %get-tuple-element.181, s32[]{:T(128)} %get-tuple-element.168), kind=kOutput, calls=%fused_computation.1.clone.1 | convolution fusion | flops 306706944 | bytes 10426880 | tf_op jit(solution)/shard_map/while/body/eval_jaxpr/qhcd,khcd->hcqk/dot_general | solution.py:75
  346.2 5.4 %fusion.55 = f32[2,2,384]{2,1,0:T(2,128)S(1)} fusion(f32[2,2,1536,384]{3,2,1,0:T(8,128)} %get-tuple-element.156, f32[2,2,384]{2,1,0:T(2,128)S(1)} %fusion.54), kind=kLoop, calls=%fused_computation.4.clone.1 | loop fusion | flops 7076352 | bytes 9449472 | tf_op jit(solution)/shard_map/while/body/eval_jaxpr/reduce_sum | solution.py:81
  351.6 1.6 constant_dynamic-slice_fusion.2
  353.2 2.6 fusion.57
  355.9 6.2 %bitcast_reduce_fusion.2 = (f32[2,2,384]{2,1,0:T(2,128)S(1)}, f32[2,2,1536,384]{3,2,1,0:T(8,128)}) fusion(bf16[384,2,2,64]{0,3,2,1:T(8,128)(2,1)S(1)} %get-tuple-element.182, bf16[8,1536,2,2,64]{1,4,3,2,0:T(8,128)(2,1)} %get-tuple-element.181, s32[]{:T(128)} %get-tuple-element.168), kind=kOutput, calls=%fused_computation.1.clone.1 | convolution fusion | flops 306706944 | bytes 10426880 | tf_op jit(solution)/shard_map/while/body/eval_jaxpr/qhcd,khcd->hcqk/dot_general | solution.py:75
  362.1 5.4 %fusion.55 = f32[2,2,384]{2,1,0:T(2,128)S(1)} fusion(f32[2,2,1536,384]{3,2,1,0:T(8,128)} %get-tuple-element.156, f32[2,2,384]{2,1,0:T(2,128)S(1)} %fusion.54), kind=kLoop, calls=%fused_computation.4.clone.1 | loop fusion | flops 7076352 | bytes 9449472 | tf_op jit(solution)/shard_map/while/body/eval_jaxpr/reduce_sum | solution.py:81
  367.5 1.6 constant_dynamic-slice_fusion.2
  369.1 2.6 fusion.57
  371.8 6.2 %bitcast_reduce_fusion.2 = (f32[2,2,384]{2,1,0:T(2,128)S(1)}, f32[2,2,1536,384]{3,2,1,0:T(8,128)}) fusion(bf16[384,2,2,64]{0,3,2,1:T(8,128)(2,1)S(1)} %get-tuple-element.182, bf16[8,1536,2,2,64]{1,4,3,2,0:T(8,128)(2,1)} %get-tuple-element.181, s32[]{:T(128)} %get-tuple-element.168), kind=kOutput, calls=%fused_computation.1.clone.1 | convolution fusion | flops 306706944 | bytes 10426880 | tf_op jit(solution)/shard_map/while/body/eval_jaxpr/qhcd,khcd->hcqk/dot_general | solution.py:75
  378.0 5.4 %fusion.55 = f32[2,2,384]{2,1,0:T(2,128)S(1)} fusion(f32[2,2,1536,384]{3,2,1,0:T(8,128)} %get-tuple-element.156, f32[2,2,384]{2,1,0:T(2,128)S(1)} %fusion.54), kind=kLoop, calls=%fused_computation.4.clone.1 | loop fusion | flops 7076352 | bytes 9449472 | tf_op jit(solution)/shard_map/while/body/eval_jaxpr/reduce_sum | solution.py:81
  383.4 1.6 constant_dynamic-slice_fusion.2
  385.0 2.6 fusion.57
  389.0 27.1 %all_to_all.24 = bf16[8,48,2048]{2,1,0:T(8,128)(2,1)S(1)} all-to-all(bf16[8,48,2048]{2,1,0:T(8,128)(2,1)S(1)} %bitcast.71), channel_id=1, replica_groups=mesh['sp'=32,'tp'=8] {'tp'}, dimensions={0} | all-to-all | bytes 3145728 | tf_op jit(solution)/shard_map/all_to_all | solution.py:19
  416.8 24.7 %all_to_all.25 = bf16[8,48,2048]{2,1,0:T(8,128)(2,1)} all-to-all(bf16[8,48,2048]{2,1,0:T(8,128)(2,1)S(1)} %broadcast_in_dim.13), channel_id=1, replica_groups=mesh['sp'=32,'tp'=8] {'tp'}, dimensions={0} | all-to-all | bytes 3145728 | tf_op jit(solution)/shard_map/all_to_all | solution.py:25
  441.5 4.1 fusion.21
  445.6 8.9 %fusion.23 = bf16[384,2048]{1,0:T(8,128)(2,1)} fusion(bf16[2048,2112]{1,0:T(8,128)(2,1)} %all-gather.5.cloned.1.call-done, bf16[384,2048]{1,0:T(8,128)(2,1)} %bitcast.73, f32[384,704]{0,1:T(8,128)S(1)} %fusion.21), kind=kOutput, calls=%fused_computation.30 | convolution fusion | flops 2217000960 | bytes 10518528 | tf_op jit(solution)/shard_map/dot_general | solution.py:136
  454.5 25.1 %all_to_all.26 = bf16[8,48,2048]{2,1,0:T(8,128)(2,1)S(1)} all-to-all(bf16[8,48,2048]{2,1,0:T(8,128)(2,1)} %bitcast.74), channel_id=1, replica_groups=mesh['sp'=32,'tp'=8] {'tp'}, dimensions={0} | all-to-all | bytes 3145728 | tf_op jit(solution)/shard_map/all_to_all | solution.py:19
  479.8 0.7 add_convert_fusion
  (100 shorter events, 3.6 us)
Async XLA Ops:
  6.5 381.8 %copy-start = (bf16[256,2048]{1,0:T(8,128)(2,1)S(1)}, bf16[256,2048]{1,0:T(8,128)(2,1)}, u32[]{:S(2)}) copy-start(bf16[256,2048]{1,0:T(8,128)(2,1)} %param.19) | copy-start | bytes 3145732
  6.5 15.9 %copy-start.2 = (bf16[384,256]{1,0:T(8,128)(2,1)S(1)}, bf16[384,256]{1,0:T(8,128)(2,1)}, u32[]{:S(2)}) copy-start(bf16[384,256]{1,0:T(8,128)(2,1)} %param.15) | copy-start | bytes 589828
  6.5 243.8 %all-gather.3.cloned.1.call-start = ((), (), s32[]{:S(2)}) async-start(), calls=%async_computation.4 | async-start | bytes 6488064 | tf_op jit(solution)/shard_map/all_gather | solution.py:102
  22.8 2.6 copy-start.3
  34.0 12.3 %copy-start.6 = (bf16[64,704]{1,0:T(8,128)(2,1)S(1)}, bf16[64,704]{1,0:T(8,128)(2,1)}, u32[]{:S(2)}) copy-start(bf16[64,704]{1,0:T(8,128)(2,1)} %param.21) | copy-start | bytes 270340
  34.0 12.3 %copy-start.7 = (bf16[64,704]{1,0:T(8,128)(2,1)S(1)}, bf16[64,704]{1,0:T(8,128)(2,1)}, u32[]{:S(2)}) copy-start(bf16[64,704]{1,0:T(8,128)(2,1)} %param.22) | copy-start | bytes 270340
  34.0 12.3 %copy-start.8 = (bf16[704,64]{0,1:T(8,128)(2,1)S(1)}, bf16[704,64]{0,1:T(8,128)(2,1)}, u32[]{:S(2)}) copy-start(bf16[704,64]{0,1:T(8,128)(2,1)} %param.23) | copy-start | bytes 270340
  34.0 13.2 %copy-start.5 = (bf16[384,256]{1,0:T(8,128)(2,1)S(1)}, bf16[384,256]{1,0:T(8,128)(2,1)}, u32[]{:S(2)}) copy-start(bf16[384,256]{1,0:T(8,128)(2,1)} %param.14) | copy-start | bytes 589828
  34.0 188.5 %all-to-all-start = ((bf16[32,384,256]{1,2,0:T(8,128)(2,1)}), bf16[32,384,256]{1,2,0:T(8,128)(2,1)}, u32[]{:S(2)}, u32[]{:S(2)}) async-start(bf16[32,384,256]{1,2,0:T(8,128)(2,1)} %copy.32), calls=%async_computation | async-start | bytes 12582912 | tf_op jit(solution)/shard_map/all_to_all | solution.py:95
  46.3 395.3 %all-gather.5.cloned.1.call-start = ((), (), s32[]{:S(2)}) async-start(), calls=%async_computation.5 | async-start | bytes 9191424 | tf_op jit(solution)/shard_map/all_gather | solution.py:43
  260.1 128.0 %copy-start.10 = (f32[2]{0:T(128)S(1)}, f32[2]{0:T(128)}, u32[]{:S(2)}) copy-start(f32[2]{0:T(128)} %param.17) | copy-start | bytes 28
  260.1 128.1 %copy-start.11 = (f32[128]{0:T(128)S(1)}, f32[128]{0:T(128)}, u32[]{:S(2)}) copy-start(f32[128]{0:T(128)} %param.18) | copy-start | bytes 1540
  266.3 7.3 %copy-start.1 = (f32[2,2,1536,384]{3,2,1,0:T(8,128)S(1)}, f32[2,2,1536,384]{3,2,1,0:T(8,128)}, u32[]{:S(2)}) copy-start(f32[2,2,1536,384]{3,2,1,0:T(8,128)} %get-tuple-element.156) | copy-start | bytes 28311556 | tf_op jit(solution)/shard_map/while
  282.5 7.1 %copy-start.1 = (f32[2,2,1536,384]{3,2,1,0:T(8,128)S(1)}, f32[2,2,1536,384]{3,2,1,0:T(8,128)}, u32[]{:S(2)}) copy-start(f32[2,2,1536,384]{3,2,1,0:T(8,128)} %get-tuple-element.156) | copy-start | bytes 28311556 | tf_op jit(solution)/shard_map/while
  298.6 7.0 %copy-start.1 = (f32[2,2,1536,384]{3,2,1,0:T(8,128)S(1)}, f32[2,2,1536,384]{3,2,1,0:T(8,128)}, u32[]{:S(2)}) copy-start(f32[2,2,1536,384]{3,2,1,0:T(8,128)} %get-tuple-element.156) | copy-start | bytes 28311556 | tf_op jit(solution)/shard_map/while
  314.5 7.0 %copy-start.1 = (f32[2,2,1536,384]{3,2,1,0:T(8,128)S(1)}, f32[2,2,1536,384]{3,2,1,0:T(8,128)}, u32[]{:S(2)}) copy-start(f32[2,2,1536,384]{3,2,1,0:T(8,128)} %get-tuple-element.156) | copy-start | bytes 28311556 | tf_op jit(solution)/shard_map/while
  330.3 7.0 %copy-start.1 = (f32[2,2,1536,384]{3,2,1,0:T(8,128)S(1)}, f32[2,2,1536,384]{3,2,1,0:T(8,128)}, u32[]{:S(2)}) copy-start(f32[2,2,1536,384]{3,2,1,0:T(8,128)} %get-tuple-element.156) | copy-start | bytes 28311556 | tf_op jit(solution)/shard_map/while
  346.2 7.0 %copy-start.1 = (f32[2,2,1536,384]{3,2,1,0:T(8,128)S(1)}, f32[2,2,1536,384]{3,2,1,0:T(8,128)}, u32[]{:S(2)}) copy-start(f32[2,2,1536,384]{3,2,1,0:T(8,128)} %get-tuple-element.156) | copy-start | bytes 28311556 | tf_op jit(solution)/shard_map/while
  362.1 7.0 %copy-start.1 = (f32[2,2,1536,384]{3,2,1,0:T(8,128)S(1)}, f32[2,2,1536,384]{3,2,1,0:T(8,128)}, u32[]{:S(2)}) copy-start(f32[2,2,1536,384]{3,2,1,0:T(8,128)} %get-tuple-element.156) | copy-start | bytes 28311556 | tf_op jit(solution)/shard_map/while
  378.0 7.0 %copy-start.1 = (f32[2,2,1536,384]{3,2,1,0:T(8,128)S(1)}, f32[2,2,1536,384]{3,2,1,0:T(8,128)}, u32[]{:S(2)}) copy-start(f32[2,2,1536,384]{3,2,1,0:T(8,128)} %get-tuple-element.156) | copy-start | bytes 28311556 | tf_op jit(solution)/shard_map/while
  387.7 28.6 %copy-start.4 = (bf16[48,2048]{1,0:T(8,128)(2,1)S(1)}, bf16[48,2048]{1,0:T(8,128)(2,1)}, u32[]{:S(2)}) copy-start(bf16[48,2048]{1,0:T(8,128)(2,1)} %param.13) | copy-start | bytes 589828
  388.0 28.5 %copy-start.9 = (f32[2048]{0:T(1024)S(1)}, f32[2048]{0:T(1024)}, u32[]{:S(2)}) copy-start(f32[2048]{0:T(1024)} %param.20) | copy-start | bytes 24580
Sparse Core Ops, SparseCore 0:
  9.9 168.3 all-gather.2
  180.8 111.7 all-gather.4
